TPU v7x, 512 devices: a whole 4x4x16 slice. The times are simulated.
512 devices in a mesh: ep: 128 (over z, x, core), tp: 4 (over y).
Axes of the slice: x: 4, y: 4, z: 16, core: 2. Of those that a mesh axis runs over, the one named last changes fastest.
Arguments:
- residual_in: bfloat16 [1920, 1536], P('ep'), may hold values from -6 to 6
- rec_state: bfloat16 [1920, 12, 128, 128], P('ep', 'tp'), may hold values from -6 to 6
- mix_gain: float32 [1536], replicated, may hold values from 0.1 to 1.9
- w_query: bfloat16 [1536, 1536], P('tp', 'ep'), may hold values from -0.15625 to 0.15625
- w_forget: bfloat16 [1536, 1536], P('tp', 'ep'), may hold values from -0.15625 to 0.15625
- w_input: bfloat16 [1536, 1536], P('tp', 'ep'), may hold values from -0.15625 to 0.15625
- w_gate: bfloat16 [1536, 1536], P('tp', 'ep'), may hold values from -0.15625 to 0.15625
- lower_bound: float32 [1536], P('tp'), may hold values from 0 to 0.9
- head_gain: float32 [128], replicated, may hold values from 0.1 to 1.9
- w_out: bfloat16 [1536, 1536], P('tp', 'ep'), may hold values from -0.15625 to 0.15625
- ffn_gain: float32 [1536], replicated, may hold values from 0.1 to 1.9
- route_ids: int32 [1920, 6], P('ep'), may hold values from 0 to 127, all different within a row; in each aligned block of 15 rows (0 to 14, 15 to 29, ...) at most 2 rows name the same one
- route_weight: float32 [1920, 6], P('ep'), may hold values from 0.2 to 1
- expert_gate: bfloat16 [128, 1536, 512], P('ep', None, 'tp'), may hold values from -0.15625 to 0.15625
- expert_up: bfloat16 [128, 1536, 512], P('ep', None, 'tp'), may hold values from -0.15625 to 0.15625
- expert_down: bfloat16 [128, 512, 1536], P('ep', 'tp'), may hold values from -0.25 to 0.25
Outputs:
- layer_out: bfloat16 [1920, 1536], P('ep', 'tp')
- new_state: bfloat16 [1920, 12, 128, 128], P('ep', 'tp')
Inputs may be any that keep to these rules, and one draw needn't show every extreme that they name: `route_ids`: each row names 6 different experts. Among the rows of one device no expert is named more than 2 times, and in every draw some device names some expert exactly 2 times.
All inputs are finite; a program needn't handle non-finite values.
Results may differ from a plain program's by a relative error of at most 0.016.
Values may be sent and summed in bfloat16 or wider, within the bound.
A program may use at most 64 MiB of HBM per device.

v0:
```python
import jax
import jax.numpy as jnp
from jax import lax
from jax.sharding import Mesh
from jax.sharding import PartitionSpec as P

EP = ("ep_0", "ep_1", "ep_2")
rms_eps = 1e-06


def in_order(pieces, dim):
    pieces = jnp.moveaxis(pieces, 0, dim)
    shape = pieces.shape
    return pieces.reshape(*shape[:dim], shape[dim] * shape[dim + 1], *shape[dim + 2 :])


def gather_in_order(x, axes, turns):
    pieces = x[None]
    for k in turns:
        pieces = lax.all_gather(pieces, axes[k], axis=0, tiled=True)
    carried = [lax.axis_size(axes[k]) for k in reversed(turns)]
    pieces = pieces.reshape(*carried, *x.shape)
    turned = sorted(range(len(turns)), key=lambda place: turns[len(turns) - 1 - place])
    return pieces.transpose(*turned, *range(len(turns), pieces.ndim)).reshape(-1, *x.shape)


def gather_axes(x, axes, turns, dim):
    return in_order(gather_in_order(x, axes, turns), dim)


def split_up(x, dim, count):
    shape = x.shape
    pieces = x.reshape(*shape[:dim], count, shape[dim] // count, *shape[dim + 1 :])
    return jnp.moveaxis(pieces, dim, 0)


def sent_and_summed(x, axis, dim):
    pieces = split_up(x, dim, lax.axis_size(axis))
    arrived = lax.all_to_all(pieces, axis, split_axis=0, concat_axis=0, tiled=True)
    return arrived.sum(axis=0)


def rms_scale(values, gain):
    return values * lax.rsqrt(jnp.mean(values * values, axis=-1, keepdims=True) + rms_eps) * gain


def rounded(values):
    return lax.optimization_barrier(values.astype(jnp.bfloat16)).astype(jnp.float32)


def recurrence(lower_bound, head_gain, state_block, query_raw, forget_raw, input_raw, gate_raw):
    seq_count = state_block.shape[0]
    heads_local = state_block.shape[1]
    head_size = state_block.shape[2]
    head_shape = (seq_count, heads_local, head_size)
    forget = lower_bound + (1.0 - lower_bound) * jax.nn.sigmoid(forget_raw)
    query_act = jax.nn.silu(query_raw).reshape(head_shape)
    key_act = (1.0 - forget).reshape(head_shape)
    forget_heads = forget.reshape(head_shape)
    value_act = input_raw.reshape(head_shape)
    state_next = (
        forget_heads[:, :, :, None] * state_block.astype(jnp.float32)
        + key_act[:, :, :, None] * value_act[:, :, None, :]
    )
    readout = jnp.einsum("shk,shkv->shv", query_act, state_next, precision=lax.Precision.HIGHEST)
    gate_heads = jax.nn.silu(gate_raw).reshape(head_shape)
    heads_out = rms_scale(readout, head_gain) * gate_heads
    return (
        state_next.astype(jnp.bfloat16),
        heads_out.reshape(seq_count, heads_local * head_size).astype(jnp.bfloat16),
    )


def shards(
    residual_in,
    rec_state,
    mix_gain,
    w_query,
    w_forget,
    w_input,
    w_gate,
    lower_bound,
    head_gain,
    w_out,
    ffn_gain,
    route_ids,
    route_weight,
    expert_gate,
    expert_up,
    expert_down,
):
    tp_count = lax.axis_size("tp")
    tp_rank = lax.axis_index("tp")
    ep_count = lax.axis_size(EP)
    seq_count = residual_in.shape[0]
    model_width = residual_in.shape[1]
    quarter = model_width // tp_count
    residual = residual_in.astype(jnp.float32)
    normed = rms_scale(residual, mix_gain).astype(jnp.bfloat16)
    own_rows = lax.dynamic_slice_in_dim(normed, tp_rank * quarter, quarter, 1)
    rows_piece = gather_axes(own_rows, EP, (0, 1, 2), 0)
    partial_proj = jnp.stack(
        [
            jnp.dot(rows_piece, weight, preferred_element_type=jnp.float32)
            for weight in (w_query, w_forget, w_input, w_gate)
        ],
        axis=1,
    )
    arrived = lax.all_to_all(
        partial_proj.astype(jnp.bfloat16), EP, split_axis=0, concat_axis=2, tiled=True
    ).astype(partial_proj.dtype)
    summed = sent_and_summed(arrived, "tp", 2)
    projected = rounded(summed)
    new_state, heads_out = recurrence(
        lower_bound,
        head_gain,
        rec_state,
        projected[:, 0],
        projected[:, 1],
        projected[:, 2],
        projected[:, 3],
    )
    partial_mix = jnp.dot(
        gather_axes(heads_out, EP, (0, 1, 2), 0), w_out, preferred_element_type=jnp.float32
    )
    mixed_home = lax.all_to_all(
        partial_mix.astype(jnp.bfloat16), EP, split_axis=0, concat_axis=1, tiled=True
    ).astype(partial_mix.dtype)
    mixed = lax.psum(mixed_home.astype(jnp.bfloat16), "tp").astype(jnp.float32)
    after_mix = rounded(residual + mixed)
    normed_ffn = rms_scale(after_mix, ffn_gain).astype(jnp.bfloat16)
    exp_dev = expert_gate.shape[0]
    experts_all = ep_count * exp_dev
    top_count = route_ids.shape[1]
    capacity = max(2, seq_count * top_count // experts_all + 1)
    flat_ids = route_ids.reshape(-1)
    onehot = (flat_ids[:, None] == jnp.arange(experts_all, dtype=jnp.int32)[None, :]).astype(
        jnp.int32
    )
    slot_rank = jnp.sum(jnp.cumsum(onehot, axis=0) * onehot, axis=1) - 1
    slot_index = flat_ids * capacity + slot_rank
    placer_int = (
        jnp.arange(experts_all * capacity, dtype=jnp.int32)[:, None] == slot_index[None, :]
    ).astype(jnp.int32)
    placer = jnp.sum(
        placer_int.reshape(experts_all * capacity, seq_count, top_count), axis=2
    ).astype(jnp.bfloat16)
    buffer = (
        jnp.dot(placer, normed_ffn, preferred_element_type=jnp.float32)
        .astype(jnp.bfloat16)
        .reshape(experts_all, capacity, model_width)
    )
    down_quarter = lax.all_to_all(expert_down, "tp", split_axis=2, concat_axis=1, tiled=True)
    own_quarter = lax.dynamic_slice_in_dim(buffer, tp_rank * quarter, quarter, 2)
    received = lax.all_gather(
        lax.all_to_all(own_quarter, EP, split_axis=0, concat_axis=0, tiled=True),
        "tp",
        axis=2,
        tiled=True,
    )
    slot_count = received.shape[1]
    grouped = received.reshape(ep_count, exp_dev, slot_count, model_width)
    gate_part = jnp.einsum(
        "sjnd,jdf->sjnf", grouped, expert_gate, preferred_element_type=jnp.float32
    )
    up_part = jnp.einsum("sjnd,jdf->sjnf", grouped, expert_up, preferred_element_type=jnp.float32)
    hidden = (jax.nn.silu(gate_part) * up_part).astype(jnp.bfloat16)
    hidden_whole = lax.all_gather(hidden, "tp", axis=3, tiled=True)
    summed_down = jnp.einsum(
        "sjnf,jfd->sjnd", hidden_whole, down_quarter, preferred_element_type=jnp.float32
    )
    returned = summed_down.astype(jnp.bfloat16).reshape(experts_all, slot_count, quarter)
    gathered_back = lax.all_to_all(returned, EP, split_axis=0, concat_axis=0, tiled=True)
    flat_back = gathered_back.reshape(experts_all * capacity, quarter)
    picked = (
        jnp.take(flat_back, slot_index, axis=0)
        .astype(jnp.float32)
        .reshape(seq_count, top_count, quarter)
    )
    expert_sum = jnp.sum(route_weight[:, :, None] * picked, axis=1)
    own_mix = lax.dynamic_slice_in_dim(after_mix, tp_rank * quarter, quarter, 1)
    layer_out = (own_mix + expert_sum).astype(jnp.bfloat16)
    return (layer_out, new_state)


def solution(mesh):
    split = Mesh(mesh.devices.reshape(16, 4, 2, mesh.shape["tp"]), ("ep_0", "ep_1", "ep_2", "tp"))
    in_specs = (
        P(EP, None),
        P(EP, "tp", None, None),
        P(),
        P("tp", EP),
        P("tp", EP),
        P("tp", EP),
        P("tp", EP),
        P("tp"),
        P(),
        P("tp", EP),
        P(),
        P(EP, None),
        P(EP, None),
        P(EP, None, "tp"),
        P(EP, None, "tp"),
        P(EP, "tp", None),
    )
    out_specs = (P(EP, "tp"), P(EP, "tp", None, None))
    return jax.shard_map(
        shards, mesh=split, in_specs=in_specs, out_specs=out_specs, check_vma=False
    )
```

profile of v0, /device:TPU:33, one launch (start us, length us, event | category | flops | bytes accessed | tf_op | source)
XLA Modules:
  0.0 379.6 jit_solution(7095298848502232704)
XLA Ops:
  9.9 27.1 %all-gather.1 = bf16[16,15,384]{2,1,0:T(8,128)(2,1)S(1)} all-gather(bf16[1,15,384]{2,1,0:T(8,128)(2,1)S(1)} %fusion.28), channel_id=2, replica_groups=mesh['ep_0'=16,'ep_1'=4,'ep_2'=2,'tp'=4] {'ep_0'}, dimensions={0}, use_global_device_ids=true | all-gather | bytes 195840 | tf_op jit(solution)/shard_map/all_gather | solution.py:20
  37.1 11.4 %all_gather.25 = bf16[64,15,384]{2,0,1:T(8,128)(2,1)} all-gather(bf16[16,15,384]{2,0,1:T(8,128)(2,1)S(1)} %copy.112), channel_id=1, replica_groups=mesh['ep_0'=16,'ep_1'=4,'ep_2'=2,'tp'=4] {'ep_1'}, dimensions={0}, use_global_device_ids=true | all-gather | bytes 921600 | tf_op jit(solution)/shard_map/all_gather | solution.py:20
  48.5 27.9 %all-gather.5.cloned.1.call-done = bf16[128,15,384]{2,0,1:T(8,128)(2,1)} async-done(((bf16[64,15,384]{2,0,1:T(8,128)(2,1)}), bf16[128,15,384]{2,0,1:T(8,128)(2,1)}) %all-gather.5.cloned.1.call-update) | async-done | bytes 1474576 | tf_op jit(solution)/shard_map/all_gather | solution.py:20
  76.4 2.2 copy.113
  81.7 1.3 copy.114
  83.0 2.1 reshape.247
  85.2 35.9 %all_to_all.58 = bf16[128,2,360]{2,1,0:T(2,128)(2,1)S(1)} all-to-all(bf16[128,2,360]{2,1,0:T(2,128)(2,1)S(1)} %reshape.247), channel_id=1, replica_groups=mesh['ep_0'=16,'ep_1'=4,'ep_2'=2,'tp'=4] {'ep_0','ep_1','ep_2'}, dimensions={0} | all-to-all | bytes 368640 | tf_op jit(solution)/shard_map/all_to_all | solution.py:109
  121.0 1.1 reshape.248
  122.1 2.0 copy.115
  124.1 4.1 %reshape.222 = f32[128,15,4,12]{1,0,2,3:T(8,128)S(1)} reshape(bf16[1920,4,12]{0,1,2:T(4,128)(2,1)} %copy.115) | data formatting | bytes 552960 | tf_op jit(solution)/shard_map/transpose | solution.py:34
  128.3 6.1 %copy.116 = f32[15,4,128,12]{3,2,1,0:T(8,128)} copy(f32[15,4,128,12]{0,2,1,3:T(8,128)S(1)} %bitcast.98) | data formatting | bytes 737280 | tf_op jit(solution)/shard_map/transpose | solution.py:34
  134.4 4.8 %reshape.221 = f32[15,4,4,384]{3,2,1,0:T(4,128)S(1)} reshape(f32[15,4,128,12]{3,2,1,0:T(8,128)} %copy.116) | data formatting | bytes 737280 | tf_op jit(solution)/shard_map/transpose | solution.py:34
  140.1 4.0 %all-to-all-start.1 = ((f32[4,15,4,384]{3,2,1,0:T(4,128)}), f32[4,15,4,384]{3,2,1,0:T(4,128)S(1)}, u32[]{:S(2)}, u32[]{:S(2)}) async-start(f32[4,15,4,384]{3,2,1,0:T(4,128)} %copy.117), calls=%async_computation.1 | async-start | bytes 737280 | tf_op jit(solution)/shard_map/all_to_all | solution.py:39
  144.1 6.9 %all-to-all-done.1 = f32[4,15,4,384]{3,2,1,0:T(4,128)S(1)} async-done(((f32[4,15,4,384]{3,2,1,0:T(4,128)}), f32[4,15,4,384]{3,2,1,0:T(4,128)S(1)}, u32[]{:S(2)}, u32[]{:S(2)}) %all-to-all-start.1) | async-done | bytes 368672 | tf_op jit(solution)/shard_map/all_to_all | solution.py:39
  151.5 4.0 %fusion.1 = f32[15,3,1,128]{3,2,1,0:T(1,128)S(1)} fusion(bf16[15,3,128,128]{3,2,1,0:T(8,128)(2,1)S(1)} %copy-done.1, f32[15,3,128]{2,1,0:T(4,128)S(1)} %mul.168, f32[15,3,128]{2,1,0:T(4,128)S(1)} %get-tuple-element.8, f32[15,3,128]{2,1,0:T(4,128)S(1)} %get-tuple-element.9, f32[15,3,128,1]{2,1,0,3:T(4,128)S(1)} %fusion.21), kind=kOutput, calls=%fused_computation.3 | convolution fusion | flops 11796480 | bytes 1589760 | tf_op jit(solution)/shard_map/shk,shkv->shv/dot_general | solution.py:65
  155.7 19.8 %all_gather.27 = bf16[16,15,384]{2,1,0:T(8,128)(2,1)S(1)} all-gather(bf16[1,15,384]{2,1,0:T(8,128)(2,1)S(1)} %convert_element_type.98), channel_id=1, replica_groups=mesh['ep_0'=16,'ep_1'=4,'ep_2'=2,'tp'=4] {'ep_0'}, dimensions={0}, use_global_device_ids=true | all-gather | bytes 195840 | tf_op jit(solution)/shard_map/all_gather | solution.py:20
  175.6 11.5 %all_gather.28 = bf16[64,15,384]{2,0,1:T(8,128)(2,1)} all-gather(bf16[16,15,384]{2,0,1:T(8,128)(2,1)S(1)} %copy.119), channel_id=1, replica_groups=mesh['ep_0'=16,'ep_1'=4,'ep_2'=2,'tp'=4] {'ep_1'}, dimensions={0}, use_global_device_ids=true | all-gather | bytes 921600 | tf_op jit(solution)/shard_map/all_gather | solution.py:20
  187.8 22.7 %all-gather.7.cloned.1.call-done = bf16[128,15,384]{2,0,1:T(8,128)(2,1)} async-done(((bf16[64,15,384]{2,0,1:T(8,128)(2,1)}), bf16[128,15,384]{2,0,1:T(8,128)(2,1)}) %all-gather.7.cloned.1.call-update) | async-done | bytes 1474576 | tf_op jit(solution)/shard_map/all_gather | solution.py:20
  210.4 2.2 copy.149
  213.2 1.2 convolution_convert_fusion.1
  216.3 16.2 %all-to-all-start.2 = ((bf16[128,15,12]{1,2,0:T(8,128)(2,1)}), bf16[128,15,12]{1,2,0:T(8,128)(2,1)S(1)}, u32[]{:S(2)}, u32[]{:S(2)}) async-start(bf16[128,15,12]{1,2,0:T(8,128)(2,1)} %copy.121), calls=%async_computation.2 | async-start | bytes 1048576 | tf_op jit(solution)/shard_map/all_to_all | solution.py:126
  233.7 8.8 %reduce.8 = bf16[1536,128]{1,0:T(8,128)(2,1)S(1)} reduce(bf16[1536,1,128]{2,1,0:T(2,128)(2,1)S(1)} %bitcast.100, bf16[]{:T(256)} %broadcast.193), dimensions={1}, to_apply=%bitcast.82.reduce_sub_computation | reduce | bytes 786434
  243.5 22.8 %all-to-all-done.2 = bf16[128,15,12]{1,2,0:T(8,128)(2,1)S(1)} async-done(((bf16[128,15,12]{1,2,0:T(8,128)(2,1)}), bf16[128,15,12]{1,2,0:T(8,128)(2,1)S(1)}, u32[]{:S(2)}, u32[]{:S(2)}) %all-to-all-start.2) | async-done | bytes 46112 | tf_op jit(solution)/shard_map/all_to_all | solution.py:126
  266.2 4.0 %all-to-all-start.4 = ((bf16[4,2,24576]{2,1,0:T(2,128)(2,1)}), bf16[4,2,24576]{2,1,0:T(2,128)(2,1)S(1)}, u32[]{:S(2)}, u32[]{:S(2)}) async-start(bf16[4,2,24576]{2,1,0:T(2,128)(2,1)} %reshape.245), calls=%async_computation.4 | async-start | bytes 786432 | tf_op jit(solution)/shard_map/all_to_all | solution.py:153
  270.6 14.8 %psum.7 = bf16[15,1536]{1,0:T(8,128)(2,1)S(1)} all-reduce(bf16[15,1536]{1,0:T(8,128)(2,1)S(1)} %copy.133), channel_id=1, replica_groups=mesh['ep_0'=16,'ep_1'=4,'ep_2'=2,'tp'=4] {'tp'}, use_global_device_ids=true, to_apply=%region_3.4 | all-reduce | flops 23040 | bytes 92160 | tf_op jit(solution)/shard_map/psum | solution.py:129
  287.1 9.6 %all-to-all-start.3 = ((bf16[128,2,384]{2,1,0:T(2,128)(2,1)}), bf16[128,2,384]{2,1,0:T(2,128)(2,1)S(1)}, u32[]{:S(2)}, u32[]{:S(2)}) async-start(bf16[128,2,384]{2,1,0:T(2,128)(2,1)} %constant_dynamic-slice_fusion), calls=%async_computation.3 | async-start | bytes 393216 | tf_op jit(solution)/shard_map/all_to_all | solution.py:156
  297.4 19.0 %all-to-all-done.3 = bf16[128,2,384]{2,1,0:T(2,128)(2,1)S(1)} async-done(((bf16[128,2,384]{2,1,0:T(2,128)(2,1)}), bf16[128,2,384]{2,1,0:T(2,128)(2,1)S(1)}, u32[]{:S(2)}, u32[]{:S(2)}) %all-to-all-start.3) | async-done | bytes 196640 | tf_op jit(solution)/shard_map/all_to_all | solution.py:156
  316.4 11.6 %all_gather.30 = bf16[128,2,1536]{2,0,1:T(8,128)(2,1)S(1)} all-gather(bf16[128,2,384]{2,0,1:T(8,128)(2,1)S(1)} %copy.127), channel_id=1, replica_groups=mesh['ep_0'=16,'ep_1'=4,'ep_2'=2,'tp'=4] {'tp'}, dimensions={2}, use_global_device_ids=true | all-gather | bytes 983040 | tf_op jit(solution)/shard_map/all_gather | solution.py:155
  328.8 9.7 %all_gather.31 = bf16[128,1,2,512]{3,0,2,1:T(8,128)(2,1)S(1)} all-gather(bf16[128,1,2,128]{3,0,2,1:T(8,128)(2,1)S(1)} %fusion.10), channel_id=1, replica_groups=mesh['ep_0'=16,'ep_1'=4,'ep_2'=2,'tp'=4] {'tp'}, dimensions={3}, use_global_device_ids=true | all-gather | bytes 327680 | tf_op jit(solution)/shard_map/all_gather | solution.py:168
  339.7 11.6 %all-to-all-start.5 = ((bf16[128,2,384]{2,1,0:T(2,128)(2,1)}), bf16[128,2,384]{2,1,0:T(2,128)(2,1)S(1)}, u32[]{:S(2)}, u32[]{:S(2)}) async-start(bf16[128,2,384]{2,1,0:T(2,128)(2,1)} %copy.130), calls=%async_computation.5 | async-start | bytes 393216 | tf_op jit(solution)/shard_map/all_to_all | solution.py:173
  351.6 2.9 fusion
  354.5 16.7 %all-to-all-done.5 = bf16[128,2,384]{2,1,0:T(2,128)(2,1)S(1)} async-done(((bf16[128,2,384]{2,1,0:T(2,128)(2,1)}), bf16[128,2,384]{2,1,0:T(2,128)(2,1)S(1)}, u32[]{:S(2)}, u32[]{:S(2)}) %all-to-all-start.5) | async-done | bytes 196640 | tf_op jit(solution)/shard_map/all_to_all | solution.py:173
  (110 shorter events, 19.0 us)
Async XLA Ops:
  7.2 320.9 %copy-start = (bf16[1,1536,128]{2,1,0:T(8,128)(2,1)S(1)}, bf16[1,1536,128]{2,1,0:T(8,128)(2,1)}, u32[]{:S(2)}) copy-start(bf16[1,1536,128]{2,1,0:T(8,128)(2,1)} %param.29) | copy-start | bytes 1179652
  7.2 69.2 %all-gather.5.cloned.1.call-start = ((), (), s32[]{:S(2)}) async-start(), calls=%async_computation.6 | async-start | bytes 2211840 | tf_op jit(solution)/shard_map/all_gather | solution.py:20
  78.7 0.7 copy-start.5
  79.4 0.7 copy-start.6
  79.4 1.2 copy-start.7
  80.1 1.0 copy-start.8
  134.4 9.7 %copy-start.10 = (f32[384]{0:T(512)S(1)}, f32[384]{0:T(512)}, u32[]{:S(2)}) copy-start(f32[384]{0:T(512)} %param.23) | copy-start | bytes 4612
  139.2 12.3 %copy-start.1 = (bf16[15,3,128,128]{3,2,1,0:T(8,128)(2,1)S(1)}, bf16[15,3,128,128]{3,2,1,0:T(8,128)(2,1)}, u32[]{:S(2)}) copy-start(bf16[15,3,128,128]{3,2,1,0:T(8,128)(2,1)} %param.17) | copy-start | bytes 4423684
  140.1 10.9 %all-to-all-start.1 = ((f32[4,15,4,384]{3,2,1,0:T(4,128)}), f32[4,15,4,384]{3,2,1,0:T(4,128)S(1)}, u32[]{:S(2)}, u32[]{:S(2)}) async-start(f32[4,15,4,384]{3,2,1,0:T(4,128)} %copy.117), calls=%async_computation.1 | async-start | bytes 737280 | tf_op jit(solution)/shard_map/all_to_all | solution.py:39
  144.1 66.4 %all-gather.7.cloned.1.call-start = ((), (), s32[]{:S(2)}) async-start(), calls=%async_computation.7 | async-start | bytes 2211840 | tf_op jit(solution)/shard_map/all_gather | solution.py:20
  151.5 4.1 %copy-start.13 = (f32[128]{0:T(128)S(1)}, f32[128]{0:T(128)}, u32[]{:S(2)}) copy-start(f32[128]{0:T(128)} %param.24) | copy-start | bytes 1540
  155.5 31.6 %copy-start.11 = (s32[15,6]{0,1:T(8,128)S(1)}, s32[15,6]{0,1:T(8,128)}, u32[]{:S(2)}) copy-start(s32[15,6]{0,1:T(8,128)} %param.27) | copy-start | bytes 1084
  187.7 22.8 %copy-start.14 = (s32[90]{0:T(128)}, s32[90]{0:T(128)S(1)}, u32[]{:S(2)}) copy-start(s32[90]{0:T(128)S(1)} %select_reduce_fusion) | copy-start | bytes 1084
  214.4 18.2 %copy-start.4 = (bf16[1,128,1536]{2,1,0:T(8,128)(2,1)S(1)}, bf16[1,128,1536]{2,1,0:T(8,128)(2,1)}, u32[]{:S(2)}) copy-start(bf16[1,128,1536]{2,1,0:T(8,128)(2,1)} %param.31) | copy-start | bytes 1179652
  216.3 50.0 %all-to-all-start.2 = ((bf16[128,15,12]{1,2,0:T(8,128)(2,1)}), bf16[128,15,12]{1,2,0:T(8,128)(2,1)S(1)}, u32[]{:S(2)}, u32[]{:S(2)}) async-start(bf16[128,15,12]{1,2,0:T(8,128)(2,1)} %copy.121), calls=%async_computation.2 | async-start | bytes 1048576 | tf_op jit(solution)/shard_map/all_to_all | solution.py:126
  242.5 42.9 %copy-start.3 = (bf16[15,1536]{1,0:T(8,128)(2,1)S(1)}, bf16[15,1536]{1,0:T(8,128)(2,1)}, u32[]{:S(2)}) copy-start(bf16[15,1536]{1,0:T(8,128)(2,1)} %param.16) | copy-start | bytes 138244
  242.5 43.0 %copy-start.9 = (f32[1536]{0:T(1024)S(1)}, f32[1536]{0:T(1024)}, u32[]{:S(2)}) copy-start(f32[1536]{0:T(1024)} %param.26) | copy-start | bytes 18436
  266.2 20.9 %all-to-all-start.4 = ((bf16[4,2,24576]{2,1,0:T(2,128)(2,1)}), bf16[4,2,24576]{2,1,0:T(2,128)(2,1)S(1)}, u32[]{:S(2)}, u32[]{:S(2)}) async-start(bf16[4,2,24576]{2,1,0:T(2,128)(2,1)} %reshape.245), calls=%async_computation.4 | async-start | bytes 786432 | tf_op jit(solution)/shard_map/all_to_all | solution.py:153
  287.1 29.3 %all-to-all-start.3 = ((bf16[128,2,384]{2,1,0:T(2,128)(2,1)}), bf16[128,2,384]{2,1,0:T(2,128)(2,1)S(1)}, u32[]{:S(2)}, u32[]{:S(2)}) async-start(bf16[128,2,384]{2,1,0:T(2,128)(2,1)} %constant_dynamic-slice_fusion), calls=%async_computation.3 | async-start | bytes 393216 | tf_op jit(solution)/shard_map/all_to_all | solution.py:156
  297.4 31.1 %copy-start.16 = (bf16[1,1536,128]{2,1,0:T(8,128)(2,1)S(1)}, bf16[1,1536,128]{2,1,0:T(8,128)(2,1)}, u32[]{:S(2)}) copy-start(bf16[1,1536,128]{2,1,0:T(8,128)(2,1)} %param.30) | copy-start | bytes 1179652
  328.4 23.0 %copy-start.12 = (f32[15,6]{0,1:T(8,128)S(1)}, f32[15,6]{0,1:T(8,128)}, u32[]{:S(2)}) copy-start(f32[15,6]{0,1:T(8,128)} %param.28) | copy-start | bytes 1084
  328.5 23.1 %copy-start.15 = (s32[90]{0:T(128)S(1)}, s32[90]{0:T(128)}, u32[]{:S(2)}) copy-start(s32[90]{0:T(128)} %copy-done.14) | copy-start | bytes 1084
  328.5 23.1 %copy-start.2 = (bf16[15,3,128,128]{3,2,1,0:T(8,128)(2,1)S(1)}, bf16[15,3,128,128]{3,2,1,0:T(8,128)(2,1)}, u32[]{:S(2)}) copy-start(bf16[15,3,128,128]{3,2,1,0:T(8,128)(2,1)} %param.17) | copy-start | bytes 4423684
  339.7 31.4 %all-to-all-start.5 = ((bf16[128,2,384]{2,1,0:T(2,128)(2,1)}), bf16[128,2,384]{2,1,0:T(2,128)(2,1)S(1)}, u32[]{:S(2)}, u32[]{:S(2)}) async-start(bf16[128,2,384]{2,1,0:T(2,128)(2,1)} %copy.130), calls=%async_computation.5 | async-start | bytes 393216 | tf_op jit(solution)/shard_map/all_to_all | solution.py:173
Sparse Core Ops, SparseCore 0:
  48.6 27.7 all-gather.4
  187.2 23.1 all-gather.6
where the time goes:
time: 381 us; the launch traced here: 380 us
  blocking collectives  142 us (37%)
  waiting for transfers between devices  116 us (30%)
  starting transfers between devices  45.5 us (12%)
  local copies, waits for them, and re-layouts  37.6 us (10%)
  other arithmetic  15.6 us (4%)
  between operations  14.5 us (4%)
  matrix products  8.61 us (2%)
    all_gather x4, blocking collectives, gather_in_order(): pieces = lax.all_gather(pieces, axes[k], axis=0, tiled=True)  69.9 us
    all_gather x2, waiting for transfers between devices, gather_in_order(): pieces = lax.all_gather(pieces, axes[k], axis=0, tiled=True)  50.6 us
    all_to_all x1, blocking collectives, shards(): lax.all_to_all(partial_proj.astype(jnp.bfloat16), EP, split_axis=0, conca...  35.9 us
    all_to_all x1, waiting for transfers between devices, shards(): lax.all_to_all(partial_mix.astype(jnp.bfloat16), EP, split_axis=0, concat...  22.8 us
    all_to_all x1, waiting for transfers between devices, shards(): lax.all_to_all(own_quarter, EP, split_axis=0, concat_axis=0, tiled=True)  19 us
    all_to_all x1, waiting for transfers between devices, shards(): lax.all_to_all(returned, EP, split_axis=0, concat_axis=0, tiled=True)  16.7 us
    all_to_all x1, starting transfers between devices, shards(): lax.all_to_all(partial_mix.astype(jnp.bfloat16), EP, split_axis=0, concat...  16.2 us
    transpose x4, local copies, waits for them, and re-layouts, split_up(): return jnp.moveaxis(pieces, dim, 0)  15.9 us
  transfers between devices with their start and end apart: 7, of which 6 were waited for; matrix products, arithmetic and copies ran while one was open for 5% of the time, Pallas kernels for 0%

commit v1 on v0

--- a/solution.py
+++ b/solution.py
@@ -17,7 +17,9 @@
 def gather_in_order(x, axes, turns):
     pieces = x[None]
     for k in turns:
-        pieces = lax.all_gather(pieces, axes[k], axis=0, tiled=True)
+        pieces = jnp.concatenate(
+            lax.all_to_all(jnp.stack([pieces] * lax.axis_size(axes[k])), axes[k], 0, 0), axis=0
+        )
     carried = [lax.axis_size(axes[k]) for k in reversed(turns)]
     pieces = pieces.reshape(*carried, *x.shape)
     turned = sorted(range(len(turns)), key=lambda place: turns[len(turns) - 1 - place])

time: 381 us -> 320 us (0.84)
  waiting for transfers between devices: 116 us -> 87.9 us
  blocking collectives: 142 us -> 124 us
  between operations: 14.5 us -> 1.23 us
    all_gather x4 -> x0, blocking collectives: 69.9 us -> none  [gather_in_order(): pieces = lax.all_gather(pieces, axes[k], axis=0, tiled=True)]
    all_to_all x0 -> x4, blocking collectives: none -> 60.1 us  [gather_in_order(): lax.all_to_all(jnp.stack([pieces] * lax.axis_size(axes[k])), axes[k], 0, 0)]
    all_gather x2 -> x0, waiting for transfers between devices: 50.6 us -> none  [gather_in_order(): pieces = lax.all_gather(pieces, axes[k], axis=0, tiled=True)]
    all_to_all x0 -> x2, waiting for transfers between devices: none -> 22.5 us  [gather_in_order(): lax.all_to_all(jnp.stack([pieces] * lax.axis_size(axes[k])), axes[k], 0, 0)]
    all_to_all x1, blocking collectives: 35.9 us -> 27.6 us  [shards(): lax.all_to_all(partial_proj.astype(jnp.bfloat16), EP, split_axis=0, conca...]
    all_to_all x1, starting transfers between devices: 16.2 us -> 8.31 us  [shards(): lax.all_to_all(partial_mix.astype(jnp.bfloat16), EP, split_axis=0, concat...]
    all_to_all x0 -> x2, starting transfers between devices: none -> 7.6 us  [gather_in_order(): lax.all_to_all(jnp.stack([pieces] * lax.axis_size(axes[k])), axes[k], 0, 0)]
    unnamed x2 -> x1, other arithmetic: 8.88 us -> 8.8 us
where the time goes in v1:
time: 320 us; the launch traced here: 319 us
  blocking collectives  124 us (39%)
  waiting for transfers between devices  87.9 us (27%)
  starting transfers between devices  44 us (14%)
  local copies, waits for them, and re-layouts  36.7 us (11%)
  other arithmetic  15.9 us (5%)
  matrix products  8.61 us (3%)
    all_to_all x4, blocking collectives, gather_in_order(): lax.all_to_all(jnp.stack([pieces] * lax.axis_size(axes[k])), axes[k], 0, 0)  60.1 us
    all_to_all x1, blocking collectives, shards(): lax.all_to_all(partial_proj.astype(jnp.bfloat16), EP, split_axis=0, conca...  27.6 us
    all_to_all x1, waiting for transfers between devices, shards(): lax.all_to_all(partial_mix.astype(jnp.bfloat16), EP, split_axis=0, concat...  22.8 us
    all_to_all x2, waiting for transfers between devices, gather_in_order(): lax.all_to_all(jnp.stack([pieces] * lax.axis_size(axes[k])), axes[k], 0, 0)  22.5 us
    all_to_all x1, waiting for transfers between devices, shards(): lax.all_to_all(own_quarter, EP, split_axis=0, concat_axis=0, tiled=True)  19 us
    all_to_all x1, waiting for transfers between devices, shards(): lax.all_to_all(returned, EP, split_axis=0, concat_axis=0, tiled=True)  16.7 us
    transpose x4, local copies, waits for them, and re-layouts, split_up(): return jnp.moveaxis(pieces, dim, 0)  15.9 us
    psum x1, blocking collectives, shards(): mixed = lax.psum(mixed_home.astype(jnp.bfloat16), 'tp').astype(jnp.float32)  15.3 us
  transfers between devices with their start and end apart: 7, of which 6 were waited for; matrix products, arithmetic and copies ran while one was open for 5% of the time, Pallas kernels for 0%

profile of v1, /device:TPU:33, one launch (start us, length us, event | category | flops | bytes accessed | tf_op | source)
XLA Modules:
  0.0 318.5 jit_solution(12783861820397967200)
XLA Ops:
  3.3 30.4 %all_to_all.88 = bf16[16,1,15,384]{3,2,1,0:T(8,128)(2,1)S(1)} all-to-all(bf16[16,1,15,384]{3,2,1,0:T(8,128)(2,1)S(1)} %stack.38), channel_id=1, replica_groups=mesh['ep_0'=16,'ep_1'=4,'ep_2'=2,'tp'=4] {'ep_0'}, dimensions={0} | all-to-all | bytes 368640 | tf_op jit(solution)/shard_map/all_to_all | solution.py:21
  33.8 14.2 %all_to_all.89 = bf16[4,16,15,384]{3,1,2,0:T(8,128)(2,1)S(1)} all-to-all(bf16[4,16,15,384]{3,1,2,0:T(8,128)(2,1)S(1)} %stack.39), channel_id=1, replica_groups=mesh['ep_0'=16,'ep_1'=4,'ep_2'=2,'tp'=4] {'ep_1'}, dimensions={0} | all-to-all | bytes 1474560 | tf_op jit(solution)/shard_map/all_to_all | solution.py:21
  48.3 6.9 %all_to_all.90 = bf16[2,64,15,384]{3,1,2,0:T(8,128)(2,1)S(1)} all-to-all(bf16[2,64,15,384]{3,1,2,0:T(8,128)(2,1)S(1)} %pad_maximum_fusion), channel_id=1, replica_groups=mesh['ep_0'=16,'ep_1'=4,'ep_2'=2,'tp'=4] {'ep_2'}, dimensions={0} | all-to-all | bytes 2949120 | tf_op jit(solution)/shard_map/all_to_all | solution.py:21
  59.1 1.3 copy.108
  60.4 2.1 reshape.239
  62.5 27.6 %all_to_all.91 = bf16[128,2,360]{2,1,0:T(2,128)(2,1)S(1)} all-to-all(bf16[128,2,360]{2,1,0:T(2,128)(2,1)S(1)} %reshape.239), channel_id=1, replica_groups=mesh['ep_0'=16,'ep_1'=4,'ep_2'=2,'tp'=4] {'ep_0','ep_1','ep_2'}, dimensions={0} | all-to-all | bytes 368640 | tf_op jit(solution)/shard_map/all_to_all | solution.py:111
  90.1 1.1 reshape.240
  91.2 2.0 copy.109
  93.2 4.1 %reshape.218 = f32[128,15,4,12]{1,0,2,3:T(8,128)S(1)} reshape(bf16[1920,4,12]{0,1,2:T(4,128)(2,1)} %copy.109) | data formatting | bytes 552960 | tf_op jit(solution)/shard_map/transpose | solution.py:36
  97.3 6.1 %copy.110 = f32[15,4,128,12]{3,2,1,0:T(8,128)} copy(f32[15,4,128,12]{0,2,1,3:T(8,128)S(1)} %bitcast.102) | data formatting | bytes 737280 | tf_op jit(solution)/shard_map/transpose | solution.py:36
  103.4 4.8 %reshape.217 = f32[15,4,4,384]{3,2,1,0:T(4,128)S(1)} reshape(f32[15,4,128,12]{3,2,1,0:T(8,128)} %copy.110) | data formatting | bytes 737280 | tf_op jit(solution)/shard_map/transpose | solution.py:36
  109.1 4.2 %all-to-all-start.4 = ((f32[4,15,4,384]{3,2,1,0:T(4,128)}), f32[4,15,4,384]{3,2,1,0:T(4,128)S(1)}, u32[]{:S(2)}, u32[]{:S(2)}) async-start(f32[4,15,4,384]{3,2,1,0:T(4,128)} %copy.111), calls=%async_computation.4 | async-start | bytes 737280 | tf_op jit(solution)/shard_map/all_to_all | solution.py:41
  113.3 6.9 %all-to-all-done.4 = f32[4,15,4,384]{3,2,1,0:T(4,128)S(1)} async-done(((f32[4,15,4,384]{3,2,1,0:T(4,128)}), f32[4,15,4,384]{3,2,1,0:T(4,128)S(1)}, u32[]{:S(2)}, u32[]{:S(2)}) %all-to-all-start.4) | async-done | bytes 368672 | tf_op jit(solution)/shard_map/all_to_all | solution.py:41
  120.7 4.0 %fusion.1 = f32[15,3,1,128]{3,2,1,0:T(1,128)S(1)} fusion(bf16[15,3,128,128]{3,2,1,0:T(8,128)(2,1)S(1)} %copy-done.1, f32[15,3,128]{2,1,0:T(4,128)S(1)} %mul.168, f32[15,3,128]{2,1,0:T(4,128)S(1)} %get-tuple-element.8, f32[15,3,128]{2,1,0:T(4,128)S(1)} %get-tuple-element.9, f32[15,3,128,1]{2,1,0,3:T(4,128)S(1)} %fusion.21), kind=kOutput, calls=%fused_computation.3 | convolution fusion | flops 11796480 | bytes 1589760 | tf_op jit(solution)/shard_map/shk,shkv->shv/dot_general | solution.py:67
  125.7 3.6 %all-to-all-start.5 = ((bf16[16,1,15,384]{3,2,1,0:T(8,128)(2,1)}), bf16[16,1,15,384]{3,2,1,0:T(8,128)(2,1)S(1)}, u32[]{:S(2)}, u32[]{:S(2)}) async-start(bf16[16,1,15,384]{3,2,1,0:T(8,128)(2,1)} %stack.46), calls=%async_computation.5 | async-start | bytes 393216 | tf_op jit(solution)/shard_map/all_to_all | solution.py:21
  129.4 14.4 %all-to-all-done.5 = bf16[16,1,15,384]{3,2,1,0:T(8,128)(2,1)S(1)} async-done(((bf16[16,1,15,384]{3,2,1,0:T(8,128)(2,1)}), bf16[16,1,15,384]{3,2,1,0:T(8,128)(2,1)S(1)}, u32[]{:S(2)}, u32[]{:S(2)}) %all-to-all-start.5) | async-done | bytes 184352 | tf_op jit(solution)/shard_map/all_to_all | solution.py:21
  144.8 4.0 %all-to-all-start.6 = ((bf16[4,16,15,384]{3,1,2,0:T(8,128)(2,1)}), bf16[4,16,15,384]{3,1,2,0:T(8,128)(2,1)S(1)}, u32[]{:S(2)}, u32[]{:S(2)}) async-start(bf16[4,16,15,384]{3,1,2,0:T(8,128)(2,1)} %stack.47), calls=%async_computation.6 | async-start | bytes 1474560 | tf_op jit(solution)/shard_map/all_to_all | solution.py:21
  149.3 8.1 %all-to-all-done.6 = bf16[4,16,15,384]{3,1,2,0:T(8,128)(2,1)S(1)} async-done(((bf16[4,16,15,384]{3,1,2,0:T(8,128)(2,1)}), bf16[4,16,15,384]{3,1,2,0:T(8,128)(2,1)S(1)}, u32[]{:S(2)}, u32[]{:S(2)}) %all-to-all-start.6) | async-done | bytes 737312 | tf_op jit(solution)/shard_map/all_to_all | solution.py:21
  157.7 8.7 %all_to_all.92 = bf16[2,64,15,384]{3,1,2,0:T(8,128)(2,1)S(1)} all-to-all(bf16[2,64,15,384]{3,1,2,0:T(8,128)(2,1)S(1)} %pad_maximum_fusion.1), channel_id=1, replica_groups=mesh['ep_0'=16,'ep_1'=4,'ep_2'=2,'tp'=4] {'ep_2'}, dimensions={0} | all-to-all | bytes 2949120 | tf_op jit(solution)/shard_map/all_to_all | solution.py:21
  167.7 1.2 convolution_convert_fusion.1
  170.8 8.3 %all-to-all-start.8 = ((bf16[128,15,12]{1,2,0:T(8,128)(2,1)}), bf16[128,15,12]{1,2,0:T(8,128)(2,1)S(1)}, u32[]{:S(2)}, u32[]{:S(2)}) async-start(bf16[128,15,12]{1,2,0:T(8,128)(2,1)} %copy.116), calls=%async_computation.8 | async-start | bytes 1048576 | tf_op jit(solution)/shard_map/all_to_all | solution.py:128
  180.3 8.8 %reduce.8 = bf16[1536,128]{1,0:T(8,128)(2,1)S(1)} reduce(bf16[1536,1,128]{2,1,0:T(2,128)(2,1)S(1)} %bitcast.105, bf16[]{:T(256)} %broadcast.199), dimensions={1}, to_apply=%bitcast.87.reduce_sub_computation | reduce | bytes 786434
  190.1 22.8 %all-to-all-done.8 = bf16[128,15,12]{1,2,0:T(8,128)(2,1)S(1)} async-done(((bf16[128,15,12]{1,2,0:T(8,128)(2,1)}), bf16[128,15,12]{1,2,0:T(8,128)(2,1)S(1)}, u32[]{:S(2)}, u32[]{:S(2)}) %all-to-all-start.8) | async-done | bytes 46112 | tf_op jit(solution)/shard_map/all_to_all | solution.py:128
  212.8 3.5 %all-to-all-start.10 = ((bf16[4,2,24576]{2,1,0:T(2,128)(2,1)}), bf16[4,2,24576]{2,1,0:T(2,128)(2,1)S(1)}, u32[]{:S(2)}, u32[]{:S(2)}) async-start(bf16[4,2,24576]{2,1,0:T(2,128)(2,1)} %reshape.237), calls=%async_computation.10 | async-start | bytes 786432 | tf_op jit(solution)/shard_map/all_to_all | solution.py:155
  216.7 15.3 %psum.7 = bf16[15,1536]{1,0:T(8,128)(2,1)S(1)} all-reduce(bf16[15,1536]{1,0:T(8,128)(2,1)S(1)} %copy.128), channel_id=1, replica_groups=mesh['ep_0'=16,'ep_1'=4,'ep_2'=2,'tp'=4] {'tp'}, use_global_device_ids=true, to_apply=%region_3.4 | all-reduce | flops 23040 | bytes 92160 | tf_op jit(solution)/shard_map/psum | solution.py:131
  233.6 8.8 %all-to-all-start.9 = ((bf16[128,2,384]{2,1,0:T(2,128)(2,1)}), bf16[128,2,384]{2,1,0:T(2,128)(2,1)S(1)}, u32[]{:S(2)}, u32[]{:S(2)}) async-start(bf16[128,2,384]{2,1,0:T(2,128)(2,1)} %constant_dynamic-slice_fusion), calls=%async_computation.9 | async-start | bytes 393216 | tf_op jit(solution)/shard_map/all_to_all | solution.py:158
  243.1 19.0 %all-to-all-done.9 = bf16[128,2,384]{2,1,0:T(2,128)(2,1)S(1)} async-done(((bf16[128,2,384]{2,1,0:T(2,128)(2,1)}), bf16[128,2,384]{2,1,0:T(2,128)(2,1)S(1)}, u32[]{:S(2)}, u32[]{:S(2)}) %all-to-all-start.9) | async-done | bytes 196640 | tf_op jit(solution)/shard_map/all_to_all | solution.py:158
  262.2 11.6 %all_gather.6 = bf16[128,2,1536]{2,0,1:T(8,128)(2,1)S(1)} all-gather(bf16[128,2,384]{2,0,1:T(8,128)(2,1)S(1)} %copy.122), channel_id=1, replica_groups=mesh['ep_0'=16,'ep_1'=4,'ep_2'=2,'tp'=4] {'tp'}, dimensions={2}, use_global_device_ids=true | all-gather | bytes 983040 | tf_op jit(solution)/shard_map/all_gather | solution.py:157
  274.6 9.7 %all_gather.7 = bf16[128,1,2,512]{3,0,2,1:T(8,128)(2,1)S(1)} all-gather(bf16[128,1,2,128]{3,0,2,1:T(8,128)(2,1)S(1)} %fusion.10), channel_id=1, replica_groups=mesh['ep_0'=16,'ep_1'=4,'ep_2'=2,'tp'=4] {'tp'}, dimensions={3}, use_global_device_ids=true | all-gather | bytes 327680 | tf_op jit(solution)/shard_map/all_gather | solution.py:170
  285.5 11.6 %all-to-all-start.11 = ((bf16[128,2,384]{2,1,0:T(2,128)(2,1)}), bf16[128,2,384]{2,1,0:T(2,128)(2,1)S(1)}, u32[]{:S(2)}, u32[]{:S(2)}) async-start(bf16[128,2,384]{2,1,0:T(2,128)(2,1)} %copy.125), calls=%async_computation.11 | async-start | bytes 393216 | tf_op jit(solution)/shard_map/all_to_all | solution.py:175
  297.4 2.9 fusion
  300.2 16.7 %all-to-all-done.11 = bf16[128,2,384]{2,1,0:T(2,128)(2,1)S(1)} async-done(((bf16[128,2,384]{2,1,0:T(2,128)(2,1)}), bf16[128,2,384]{2,1,0:T(2,128)(2,1)S(1)}, u32[]{:S(2)}, u32[]{:S(2)}) %all-to-all-start.11) | async-done | bytes 196640 | tf_op jit(solution)/shard_map/all_to_all | solution.py:175
  (117 shorter events, 22.9 us)
Async XLA Ops:
  0.6 273.2 %copy-start = (bf16[1,1536,128]{2,1,0:T(8,128)(2,1)S(1)}, bf16[1,1536,128]{2,1,0:T(8,128)(2,1)}, u32[]{:S(2)}) copy-start(bf16[1,1536,128]{2,1,0:T(8,128)(2,1)} %param.29) | copy-start | bytes 1179652
  56.0 0.7 copy-start.5
  56.7 0.7 copy-start.6
  56.7 1.2 copy-start.7
  57.4 1.0 copy-start.8
  103.4 9.9 %copy-start.10 = (f32[384]{0:T(512)S(1)}, f32[384]{0:T(512)}, u32[]{:S(2)}) copy-start(f32[384]{0:T(512)} %param.23) | copy-start | bytes 4612
  108.3 12.5 %copy-start.1 = (bf16[15,3,128,128]{3,2,1,0:T(8,128)(2,1)S(1)}, bf16[15,3,128,128]{3,2,1,0:T(8,128)(2,1)}, u32[]{:S(2)}) copy-start(bf16[15,3,128,128]{3,2,1,0:T(8,128)(2,1)} %param.17) | copy-start | bytes 4423684
  109.1 11.1 %all-to-all-start.4 = ((f32[4,15,4,384]{3,2,1,0:T(4,128)}), f32[4,15,4,384]{3,2,1,0:T(4,128)S(1)}, u32[]{:S(2)}, u32[]{:S(2)}) async-start(f32[4,15,4,384]{3,2,1,0:T(4,128)} %copy.111), calls=%async_computation.4 | async-start | bytes 737280 | tf_op jit(solution)/shard_map/all_to_all | solution.py:41
  120.7 4.1 %copy-start.13 = (f32[128]{0:T(128)S(1)}, f32[128]{0:T(128)}, u32[]{:S(2)}) copy-start(f32[128]{0:T(128)} %param.24) | copy-start | bytes 1540
  120.7 8.5 %copy-start.11 = (s32[15,6]{0,1:T(8,128)S(1)}, s32[15,6]{0,1:T(8,128)}, u32[]{:S(2)}) copy-start(s32[15,6]{0,1:T(8,128)} %param.27) | copy-start | bytes 1084
  125.7 18.1 %all-to-all-start.5 = ((bf16[16,1,15,384]{3,2,1,0:T(8,128)(2,1)}), bf16[16,1,15,384]{3,2,1,0:T(8,128)(2,1)S(1)}, u32[]{:S(2)}, u32[]{:S(2)}) async-start(bf16[16,1,15,384]{3,2,1,0:T(8,128)(2,1)} %stack.46), calls=%async_computation.5 | async-start | bytes 393216 | tf_op jit(solution)/shard_map/all_to_all | solution.py:21
  144.8 12.6 %all-to-all-start.6 = ((bf16[4,16,15,384]{3,1,2,0:T(8,128)(2,1)}), bf16[4,16,15,384]{3,1,2,0:T(8,128)(2,1)S(1)}, u32[]{:S(2)}, u32[]{:S(2)}) async-start(bf16[4,16,15,384]{3,1,2,0:T(8,128)(2,1)} %stack.47), calls=%async_computation.6 | async-start | bytes 1474560 | tf_op jit(solution)/shard_map/all_to_all | solution.py:21
  149.2 8.5 %copy-start.14 = (s32[90]{0:T(128)}, s32[90]{0:T(128)S(1)}, u32[]{:S(2)}) copy-start(s32[90]{0:T(128)S(1)} %select_reduce_fusion) | copy-start | bytes 1084
  168.9 10.3 %copy-start.4 = (bf16[1,128,1536]{2,1,0:T(8,128)(2,1)S(1)}, bf16[1,128,1536]{2,1,0:T(8,128)(2,1)}, u32[]{:S(2)}) copy-start(bf16[1,128,1536]{2,1,0:T(8,128)(2,1)} %param.31) | copy-start | bytes 1179652
  170.8 42.0 %all-to-all-start.8 = ((bf16[128,15,12]{1,2,0:T(8,128)(2,1)}), bf16[128,15,12]{1,2,0:T(8,128)(2,1)S(1)}, u32[]{:S(2)}, u32[]{:S(2)}) async-start(bf16[128,15,12]{1,2,0:T(8,128)(2,1)} %copy.116), calls=%async_computation.8 | async-start | bytes 1048576 | tf_op jit(solution)/shard_map/all_to_all | solution.py:128
  189.1 42.8 %copy-start.3 = (bf16[15,1536]{1,0:T(8,128)(2,1)S(1)}, bf16[15,1536]{1,0:T(8,128)(2,1)}, u32[]{:S(2)}) copy-start(bf16[15,1536]{1,0:T(8,128)(2,1)} %param.16) | copy-start | bytes 138244
  189.1 43.0 %copy-start.9 = (f32[1536]{0:T(1024)S(1)}, f32[1536]{0:T(1024)}, u32[]{:S(2)}) copy-start(f32[1536]{0:T(1024)} %param.26) | copy-start | bytes 18436
  212.8 20.8 %all-to-all-start.10 = ((bf16[4,2,24576]{2,1,0:T(2,128)(2,1)}), bf16[4,2,24576]{2,1,0:T(2,128)(2,1)S(1)}, u32[]{:S(2)}, u32[]{:S(2)}) async-start(bf16[4,2,24576]{2,1,0:T(2,128)(2,1)} %reshape.237), calls=%async_computation.10 | async-start | bytes 786432 | tf_op jit(solution)/shard_map/all_to_all | solution.py:155
  233.6 28.5 %all-to-all-start.9 = ((bf16[128,2,384]{2,1,0:T(2,128)(2,1)}), bf16[128,2,384]{2,1,0:T(2,128)(2,1)S(1)}, u32[]{:S(2)}, u32[]{:S(2)}) async-start(bf16[128,2,384]{2,1,0:T(2,128)(2,1)} %constant_dynamic-slice_fusion), calls=%async_computation.9 | async-start | bytes 393216 | tf_op jit(solution)/shard_map/all_to_all | solution.py:158
  243.1 31.1 %copy-start.16 = (bf16[1,1536,128]{2,1,0:T(8,128)(2,1)S(1)}, bf16[1,1536,128]{2,1,0:T(8,128)(2,1)}, u32[]{:S(2)}) copy-start(bf16[1,1536,128]{2,1,0:T(8,128)(2,1)} %param.30) | copy-start | bytes 1179652
  274.2 23.0 %copy-start.12 = (f32[15,6]{0,1:T(8,128)S(1)}, f32[15,6]{0,1:T(8,128)}, u32[]{:S(2)}) copy-start(f32[15,6]{0,1:T(8,128)} %param.28) | copy-start | bytes 1084
  274.2 23.1 %copy-start.15 = (s32[90]{0:T(128)S(1)}, s32[90]{0:T(128)}, u32[]{:S(2)}) copy-start(s32[90]{0:T(128)} %copy-done.14) | copy-start | bytes 1084
  274.2 23.1 %copy-start.2 = (bf16[15,3,128,128]{3,2,1,0:T(8,128)(2,1)S(1)}, bf16[15,3,128,128]{3,2,1,0:T(8,128)(2,1)}, u32[]{:S(2)}) copy-start(bf16[15,3,128,128]{3,2,1,0:T(8,128)(2,1)} %param.17) | copy-start | bytes 4423684
  285.5 31.4 %all-to-all-start.11 = ((bf16[128,2,384]{2,1,0:T(2,128)(2,1)}), bf16[128,2,384]{2,1,0:T(2,128)(2,1)S(1)}, u32[]{:S(2)}, u32[]{:S(2)}) async-start(bf16[128,2,384]{2,1,0:T(2,128)(2,1)} %copy.125), calls=%async_computation.11 | async-start | bytes 393216 | tf_op jit(solution)/shard_map/all_to_all | solution.py:175
